TPU v7x, 32 devices: a whole 2x2x4 slice. The times are simulated.
32 devices in a mesh: fs: 16 (over z, y, x), tp: 2 (over core).
Axes of the slice: x: 2, y: 2, z: 4, core: 2. Of those that a mesh axis runs over, the one named last changes fastest.
Arguments:
- tokens: bfloat16 [4096, 2048], P('fs', 'tp'), may hold values from -6 to 6
- mixer_norm_gain: bfloat16 [2048], replicated, may hold values from 0.099609375 to 1.8984375
- recurrence_branch_weight: bfloat16 [2048, 1024], P('fs', 'tp'), may hold values from -0.125 to 0.125
- output_gate_projection: bfloat16 [2048, 1024], P('fs', 'tp'), may hold values from -0.125 to 0.125
- recurrence_conv_taps: bfloat16 [4, 1024], P(None, 'tp'), may hold values from -3 to 3
- recurrence_gate_map: bfloat16 [16, 64, 64], P('tp'), may hold values from -0.75 to 0.75
- input_gate_map: bfloat16 [16, 64, 64], P('tp'), may hold values from -0.75 to 0.75
- channel_decay_rate: float32 [1024], P('tp'), may hold values from 0.001 to 0.03
- position_log_decay: float32 [4096, 1024], P('fs', 'tp'), may hold values from -0.69 to 0
- mixer_output_weight: bfloat16 [1024, 2048], P('tp', 'fs'), may hold values from -0.75 to 0.75
- feedforward_norm_gain: bfloat16 [2048], replicated, may hold values from 0.099609375 to 1.8984375
- gate_up_weight: bfloat16 [2048, 5632], P('fs', 'tp'), may hold values from -0.125 to 0.125
- value_up_weight: bfloat16 [2048, 5632], P('fs', 'tp'), may hold values from -0.125 to 0.125
- gate_conv_taps: bfloat16 [3, 5632], P(None, 'tp'), may hold values from -3 to 3
- value_conv_taps: bfloat16 [3, 5632], P(None, 'tp'), may hold values from -3 to 3
- down_projection_weight: bfloat16 [5632, 2048], P('tp', 'fs'), may hold values from -0.15625 to 0.15625
Outputs:
- result: bfloat16 [4096, 2048], P('fs', 'tp')
All inputs are finite; a program needn't handle non-finite values.
Results may differ from a plain program's by a relative error of at most 0.024.
Values may be sent and summed in bfloat16 or wider, within the bound.
A program may use at most 128 MiB of HBM per device.

v0:
```python
import jax
import jax.numpy as jnp
from jax import lax
from jax.sharding import PartitionSpec as P

SEQ_LEN = 64
EPS = 1e-06
DECAY_RATE_GAIN = 8.0


def rms_normed(values, gain):
    wide = values.astype(jnp.float32)
    factor = lax.rsqrt(jnp.mean(wide * wide, axis=-1, keepdims=True) + EPS)
    return (wide * factor * gain.astype(jnp.float32)).astype(jnp.bfloat16)


def causal_conv(values, kernel):
    width = kernel.shape[0]
    row_count, channels = values.shape
    grouped = values.astype(jnp.float32).reshape(row_count // SEQ_LEN, SEQ_LEN, channels)
    padded = jnp.pad(grouped, ((0, 0), (width - 1, 0), (0, 0)))
    summed = padded[:, 0:SEQ_LEN] * kernel[0].astype(jnp.float32)
    for offset in range(1, width):
        summed = summed + padded[:, offset : offset + SEQ_LEN] * kernel[offset].astype(jnp.float32)
    return summed.reshape(row_count, channels)


def combine(left, right):
    first_a, first_b = left
    second_a, second_b = right
    return (first_a * second_a, second_a * first_b + second_b)


def pair_folder(normed, pieces):
    return (
        jnp.dot(normed, pieces[0], preferred_element_type=jnp.float32),
        jnp.dot(normed, pieces[1], preferred_element_type=jnp.float32),
    )


def per_device(
    tokens,
    mixer_norm_gain,
    recurrence_branch_weight,
    output_gate_projection,
    recurrence_conv_taps,
    recurrence_gate_map,
    input_gate_map,
    channel_decay_rate,
    position_log_decay,
    mixer_output_weight,
    feedforward_norm_gain,
    gate_up_weight,
    value_up_weight,
    gate_conv_taps,
    value_conv_taps,
    down_projection_weight,
):
    row_count = tokens.shape[0]
    local_width = recurrence_branch_weight.shape[1]
    local_heads = recurrence_gate_map.shape[0]
    head_size = recurrence_gate_map.shape[1]
    whole_rows = lax.all_gather(tokens, "tp", axis=1, tiled=True)
    normed = rms_normed(whole_rows, mixer_norm_gain)
    branch_sum, outgate_sum = pair_folder(
        normed,
        (
            lax.all_gather(recurrence_branch_weight, "fs", axis=0, tiled=True),
            lax.all_gather(output_gate_projection, "fs", axis=0, tiled=True),
        ),
    )
    branch = branch_sum.astype(jnp.bfloat16)
    outgate = outgate_sum.astype(jnp.bfloat16)
    conv = causal_conv(branch, recurrence_conv_taps).astype(jnp.bfloat16)
    grouped = conv.reshape(row_count, local_heads, head_size)
    recurrence_scan = jax.nn.sigmoid(
        jnp.einsum(
            "rhi,hij->rhj", grouped, recurrence_gate_map, preferred_element_type=jnp.float32
        ).reshape(row_count, local_width)
    )
    inner = jax.nn.sigmoid(
        jnp.einsum(
            "rhi,hij->rhj", grouped, input_gate_map, preferred_element_type=jnp.float32
        ).reshape(row_count, local_width)
    )
    log_alpha = (
        -DECAY_RATE_GAIN * recurrence_scan * channel_decay_rate[None, :] + position_log_decay
    )
    drive = jnp.sqrt(-jnp.expm1(2.0 * log_alpha)) * inner * conv.astype(jnp.float32)
    shape3 = (row_count // SEQ_LEN, SEQ_LEN, local_width)
    unused, state = lax.associative_scan(
        combine, (jnp.exp(log_alpha).reshape(shape3), drive.reshape(shape3)), axis=1
    )
    state = state.reshape(row_count, local_width)
    mixed = (state * jax.nn.gelu(outgate.astype(jnp.float32))).astype(jnp.bfloat16)
    mixer_terms = jnp.dot(
        mixed,
        lax.all_gather(mixer_output_weight, "fs", axis=1, tiled=True),
        preferred_element_type=jnp.float32,
    )
    mixer_terms = mixer_terms.astype(jnp.bfloat16).astype(jnp.float32)
    mixer_whole = lax.psum(mixer_terms.astype(jnp.bfloat16), "tp").astype(jnp.float32)
    whole_after = (whole_rows.astype(jnp.float32) + mixer_whole).astype(jnp.bfloat16)
    normed2 = rms_normed(whole_after, feedforward_norm_gain)
    gate_whole, value_whole = (
        lax.all_gather(gate_up_weight, "fs", axis=0, tiled=True),
        lax.all_gather(value_up_weight, "fs", axis=0, tiled=True),
    )
    gate_sum = jnp.dot(normed2, gate_whole, preferred_element_type=jnp.float32)
    value_sum = jnp.dot(normed2, value_whole, preferred_element_type=jnp.float32)
    gate_half = gate_sum.astype(jnp.bfloat16)
    value_half = value_sum.astype(jnp.bfloat16)
    hidden = (
        jax.nn.silu(causal_conv(gate_half, gate_conv_taps))
        * causal_conv(value_half, value_conv_taps)
    ).astype(jnp.bfloat16)
    channel_terms = jnp.dot(
        hidden,
        lax.all_gather(down_projection_weight, "fs", axis=1, tiled=True),
        preferred_element_type=jnp.float32,
    )
    channel_terms = channel_terms.astype(jnp.bfloat16).astype(jnp.float32)
    channel_share = lax.psum_scatter(
        channel_terms.astype(jnp.bfloat16), "tp", scatter_dimension=1, tiled=True
    ).astype(jnp.float32)
    share_width = channel_share.shape[1]
    residual_share = lax.dynamic_slice_in_dim(
        whole_after, lax.axis_index("tp") * share_width, share_width, 1
    )
    return (residual_share.astype(jnp.float32) + channel_share).astype(jnp.bfloat16)


def solution(mesh):
    placed = (
        P("fs", "tp"),
        P(),
        P("fs", "tp"),
        P("fs", "tp"),
        P(None, "tp"),
        P("tp", None, None),
        P("tp", None, None),
        P("tp"),
        P("fs", "tp"),
        P("tp", "fs"),
        P(),
        P("fs", "tp"),
        P("fs", "tp"),
        P(None, "tp"),
        P(None, "tp"),
        P("tp", "fs"),
    )
    return jax.shard_map(
        per_device, mesh=mesh, in_specs=placed, out_specs=P("fs", "tp"), check_vma=False
    )
```

profile of v0, /device:TPU:0, one launch (start us, length us, event | category | flops | bytes accessed | tf_op | source)
XLA Modules:
  0.0 728.2 jit_solution(12462820517022480084)
XLA Ops:
  6.5 0.7 all-gather.8.cloned.1.call-update
  7.3 0.0 all-gather.10.cloned.1.call-start
  7.3 0.7 all-gather.10.cloned.1.call-update
  8.0 0.0 all-gather.12.cloned.1.call-start
  8.1 0.7 all-gather.12.cloned.1.call-update
  8.8 0.5 all-gather.14.cloned.1.call-update
  9.3 0.0 all-reduce.17.cloned.1.call-start
  9.4 0.7 convert_element_type.188
  10.1 0.8 slice_convert_fusion.3
  10.9 0.7 broadcast_multiply_fusion
  11.6 9.1 %all-gather.8.cloned.1.call-done = bf16[256,2048]{1,0:T(8,128)(2,1)} async-done(((bf16[256,1024]{1,0:T(8,128)(2,1)}), bf16[256,2048]{1,0:T(8,128)(2,1)}) %all-gather.8.cloned.1.call-update) | async-done | bytes 1048592 | tf_op jit(solution)/shard_map/all_gather | solution.py:63
  20.7 1.5 fusion.15
  22.2 62.8 %all-gather.10.cloned.1.call-done = bf16[2048,512]{1,0:T(8,128)(2,1)} async-done(((bf16[128,512]{1,0:T(8,128)(2,1)}), bf16[2048,512]{1,0:T(8,128)(2,1)}) %all-gather.10.cloned.1.call-update) | async-done | bytes 2097168 | tf_op jit(solution)/shard_map/all_gather | solution.py:68
  85.0 2.7 convolution_convert_fusion.5
  87.7 0.1 convert.14
  87.8 0.2 fusion.30
  88.0 0.3 convert_element_type.200
  88.3 0.3 copy.22
  88.6 0.4 fusion.22
  89.0 0.2 copy.24
  89.2 0.4 fusion.24
  89.6 0.2 copy.27
  89.8 0.4 fusion.52
  90.2 0.1 slice.199
  90.4 0.1 slice.200
  90.5 0.1 slice.198
  90.7 0.1 slice.202
  90.8 0.1 fusion.64
  91.8 0.1 slice.203
  91.8 0.1 slice.236
  91.9 0.2 slice.238
  92.1 0.2 slice.197
  92.4 0.1 pad.52
  92.5 0.1 pad.51
  93.0 0.1 pad.57
  93.1 0.1 pad.58
  93.2 0.1 pad.60
  93.4 0.1 fusion.47
  93.5 0.1 pad.59
  93.6 0.1 add.183
  93.7 53.3 %all-gather.12.cloned.1.call-done = bf16[2048,512]{1,0:T(8,128)(2,1)} async-done(((bf16[128,512]{1,0:T(8,128)(2,1)}), bf16[2048,512]{1,0:T(8,128)(2,1)}) %all-gather.12.cloned.1.call-update) | async-done | bytes 2097168 | tf_op jit(solution)/shard_map/all_gather | solution.py:69
  147.0 64.3 %all-gather.14.cloned.1.call-done = bf16[512,2048]{1,0:T(8,128)(2,1)} async-done(((bf16[512,128]{1,0:T(8,128)(2,1)}), bf16[512,2048]{1,0:T(8,128)(2,1)}) %all-gather.14.cloned.1.call-update) | async-done | bytes 2097168 | tf_op jit(solution)/shard_map/all_gather | solution.py:98
  211.3 4.7 convolution_convert_fusion.3
  216.1 0.0 all-gather.18.cloned.1.call-start
  216.1 0.5 all-gather.18.cloned.1.call-update
  216.7 0.7 all-gather.16.cloned.1.call-update
  217.5 0.7 all-gather.20.cloned.1.call-update
  218.2 0.2 reduce-scatter.2.cloned.1.call-start
  218.4 0.1 convert_reduce_fusion.2
  218.5 0.1 convert_reduce_fusion.5
  218.6 15.2 %all-reduce.17.cloned.1.call-done = bf16[256,2048]{1,0:T(8,128)(2,1)} async-done(((bf16[256,2048]{1,0:T(8,128)(2,1)}), bf16[256,2048]{1,0:T(8,128)(2,1)}) %all-reduce.17.cloned.1.call-update) | async-done | bytes 1048592 | tf_op jit(solution)/shard_map/psum | solution.py:102
  233.8 1.7 fusion.12
  235.6 143.5 %all-gather.18.cloned.1.call-done = bf16[2048,2816]{1,0:T(8,128)(2,1)} async-done(((bf16[128,2816]{1,0:T(8,128)(2,1)}), bf16[2048,2816]{1,0:T(8,128)(2,1)}) %all-gather.18.cloned.1.call-update) | async-done | bytes 11534352 | tf_op jit(solution)/shard_map/all_gather | solution.py:107
  379.1 7.5 %convolution_convert_fusion = bf16[256,2816]{1,0:T(8,128)(2,1)S(1)} fusion(bf16[2048,2816]{1,0:T(8,128)(2,1)} %all-gather.18.cloned.1.call-done, bf16[256,2048]{1,0:T(8,128)(2,1)S(1)} %get-tuple-element.12, f32[2048]{0:T(1024)S(1)} %convert_element_type.211, f32[256]{0:T(256)S(1)} %add_rsqrt_fusion), kind=kOutput, calls=%fused_computation | convolution fusion | flops 2955608064 | bytes 14033920 | tf_op jit(solution)/shard_map/dot_general | solution.py:110
  386.6 0.2 convert.16
  386.8 134.7 %all-gather.16.cloned.1.call-done = bf16[2048,2816]{1,0:T(8,128)(2,1)} async-done(((bf16[128,2816]{1,0:T(8,128)(2,1)}), bf16[2048,2816]{1,0:T(8,128)(2,1)}) %all-gather.16.cloned.1.call-update) | async-done | bytes 11534352 | tf_op jit(solution)/shard_map/all_gather | solution.py:106
  521.5 7.8 %convolution_convert_fusion.1 = bf16[256,2816]{1,0:T(8,128)(2,1)S(1)} fusion(bf16[2048,2816]{1,0:T(8,128)(2,1)} %all-gather.16.cloned.1.call-done, bf16[256,2048]{1,0:T(8,128)(2,1)} %copy-done.3, f32[2048]{0:T(1024)S(1)} %convert_element_type.211, f32[256]{0:T(256)S(1)} %add_rsqrt_fusion), kind=kOutput, calls=%fused_computation.1 | convolution fusion | flops 2955608064 | bytes 14033920 | tf_op jit(solution)/shard_map/dot_general | solution.py:109
  529.3 0.2 convert.15
  529.5 1.8 fusion.2
  531.3 0.8 fusion.8
  532.2 172.3 %all-gather.20.cloned.1.call-done = bf16[2816,2048]{1,0:T(8,128)(2,1)} async-done(((bf16[2816,128]{1,0:T(8,128)(2,1)}), bf16[2816,2048]{1,0:T(8,128)(2,1)}) %all-gather.20.cloned.1.call-update) | async-done | bytes 11534352 | tf_op jit(solution)/shard_map/all_gather | solution.py:119
  704.4 8.5 %convolution_convert_fusion.2 = bf16[256,2048]{1,0:T(8,128)(2,1)} fusion(bf16[256,2816]{1,0:T(8,128)(2,1)S(1)} %fusion.8, bf16[2816,2048]{1,0:T(8,128)(2,1)} %all-gather.20.cloned.1.call-done), kind=kOutput, calls=%fused_computation.26 | convolution fusion | flops 2953314304 | bytes 14024704 | tf_op jit(solution)/shard_map/dot_general | solution.py:117
  712.9 6.7 reduce-scatter.2.cloned.1.call-done
  719.7 2.0 add_convert_fusion
  (76 shorter events, 1.5 us)
Async XLA Ops:
  6.5 82.1 %copy-start = (bf16[8,64,64]{2,1,0:T(8,128)(2,1)S(1)}, bf16[8,64,64]{2,1,0:T(8,128)(2,1)}, u32[]{:S(2)}) copy-start(bf16[8,64,64]{2,1,0:T(8,128)(2,1)} %param.21) | copy-start | bytes 196612
  6.5 14.1 %all-gather.8.cloned.1.call-start = ((), (), s32[]{:S(2)}) async-start(), calls=%async_computation.1 | async-start | bytes 1572864 | tf_op jit(solution)/shard_map/all_gather | solution.py:63
  7.3 77.8 %all-gather.10.cloned.1.call-start = ((), (), s32[]{:S(2)}) async-start(), calls=%async_computation.2 | async-start | bytes 2228224 | tf_op jit(solution)/shard_map/all_gather | solution.py:68
  8.0 139.0 %all-gather.12.cloned.1.call-start = ((), (), s32[]{:S(2)}) async-start(), calls=%async_computation.3 | async-start | bytes 2228224 | tf_op jit(solution)/shard_map/all_gather | solution.py:69
  8.7 202.6 %all-gather.14.cloned.1.call-start = ((), (), s32[]{:S(2)}) async-start(), calls=%async_computation.4 | async-start | bytes 2228224 | tf_op jit(solution)/shard_map/all_gather | solution.py:98
  9.3 224.5 %all-reduce.17.cloned.1.call-start = ((), (), s32[]{:S(2)}) async-start(), calls=%async_computation.5 | async-start | bytes 2097152 | tf_op jit(solution)/shard_map/psum | solution.py:102
  87.8 1.5 copy-start.9
  88.6 1.2 copy-start.5
  93.2 118.2 %copy-start.2 = (bf16[256,2048]{1,0:T(8,128)(2,1)S(1)}, bf16[256,2048]{1,0:T(8,128)(2,1)}, u32[]{:S(2)}) copy-start(bf16[256,2048]{1,0:T(8,128)(2,1)} %all-gather.8.cloned.1.call-done) | copy-start | bytes 3145732
  216.1 2.3 copy-start.8
  216.1 2.4 copy-start.6
  216.1 2.5 copy-start.7
  216.1 163.0 %all-gather.18.cloned.1.call-start = ((), (), s32[]{:S(2)}) async-start(), calls=%async_computation.7 | async-start | bytes 12255232 | tf_op jit(solution)/shard_map/all_gather | solution.py:107
  216.7 304.8 %all-gather.16.cloned.1.call-start = ((), (), s32[]{:S(2)}) async-start(), calls=%async_computation.6 | async-start | bytes 12255232 | tf_op jit(solution)/shard_map/all_gather | solution.py:106
  217.4 487.0 %all-gather.20.cloned.1.call-start = ((), (), s32[]{:S(2)}) async-start(), calls=%async_computation.8 | async-start | bytes 12255232 | tf_op jit(solution)/shard_map/all_gather | solution.py:119
  218.2 501.5 %reduce-scatter.2.cloned.1.call-start = ((), (), s32[]{:S(2)}) async-start(), calls=%async_computation.9 | async-start | bytes 1572864 | tf_op jit(solution)/shard_map/reduce_scatter | solution.py:123
  235.6 151.0 %copy-start.3 = (bf16[256,2048]{1,0:T(8,128)(2,1)}, bf16[256,2048]{1,0:T(8,128)(2,1)S(1)}, u32[]{:S(2)}) copy-start(bf16[256,2048]{1,0:T(8,128)(2,1)S(1)} %get-tuple-element.12) | copy-start | bytes 3145732
  532.2 187.5 %copy-start.4 = (bf16[256,2048]{1,0:T(8,128)(2,1)S(1)}, bf16[256,2048]{1,0:T(8,128)(2,1)}, u32[]{:S(2)}) copy-start(bf16[256,2048]{1,0:T(8,128)(2,1)} %copy-done.3) | copy-start | bytes 3145732
  704.4 17.3 %copy-start.1 = (bf16[8,64,64]{2,1,0:T(8,128)(2,1)S(1)}, bf16[8,64,64]{2,1,0:T(8,128)(2,1)}, u32[]{:S(2)}) copy-start(bf16[8,64,64]{2,1,0:T(8,128)(2,1)} %param.21) | copy-start | bytes 196612
Sparse Core Ops, SparseCore 0:
  8.9 11.7 all-gather.7
  23.4 61.5 all-gather.9
  87.8 59.1 all-gather.11
  149.6 61.7 all-gather.13
  216.2 17.5 all-reduce.16
  236.4 142.6 all-gather.17
  381.8 139.5 all-gather.15
  524.2 180.2 all-gather.19
  713.0 6.5 reduce-scatter.1
where the time goes:
time: 729 us; the launch traced here: 728 us
  waiting for transfers between devices  666 us (91%)
  matrix products  31.8 us (4%)
  between operations  13.8 us (2%)
  other arithmetic  12.2 us (2%)
    all_gather x1, waiting for transfers between devices, per_device(): lax.all_gather(down_projection_weight, 'fs', axis=1, tiled=True)  172 us
    all_gather x1, waiting for transfers between devices, per_device(): lax.all_gather(value_up_weight, 'fs', axis=0, tiled=True)  144 us
    all_gather x1, waiting for transfers between devices, per_device(): lax.all_gather(gate_up_weight, 'fs', axis=0, tiled=True)  135 us
    all_gather x1, waiting for transfers between devices, per_device(): lax.all_gather(mixer_output_weight, 'fs', axis=1, tiled=True)  64.3 us
    all_gather x1, waiting for transfers between devices, per_device(): lax.all_gather(recurrence_branch_weight, 'fs', axis=0, tiled=True)  62.8 us
    all_gather x1, waiting for transfers between devices, per_device(): lax.all_gather(output_gate_projection, 'fs', axis=0, tiled=True)  53.3 us
    psum x1, waiting for transfers between devices, per_device(): lax.psum(mixer_terms.astype(jnp.bfloat16), 'tp').astype(jnp.float32)  15.2 us
  transfers between devices with their start and end apart: 9, of which 9 were waited for; matrix products, arithmetic and copies ran while one was open for 4% of the time, Pallas kernels for 0%

commit v1 on v0

--- a/solution.py
+++ b/solution.py
@@ -95,7 +95,10 @@
     mixed = (state * jax.nn.gelu(outgate.astype(jnp.float32))).astype(jnp.bfloat16)
     mixer_terms = jnp.dot(
         mixed,
-        lax.all_gather(mixer_output_weight, "fs", axis=1, tiled=True),
+        jnp.concatenate(
+            lax.all_to_all(jnp.stack([mixer_output_weight] * lax.axis_size("fs")), "fs", 0, 0),
+            axis=1,
+        ),
         preferred_element_type=jnp.float32,
     )
     mixer_terms = mixer_terms.astype(jnp.bfloat16).astype(jnp.float32)

time: 729 us -> 677 us (0.929)
  waiting for transfers between devices: 666 us -> 606 us
  starting transfers between devices: 0.49 us -> 8.98 us
    all_gather x1 -> x0, waiting for transfers between devices: 64.3 us -> none  [per_device(): lax.all_gather(mixer_output_weight, 'fs', axis=1, tiled=True)]
    all_gather x1, waiting for transfers between devices: 62.8 us -> 75 us  [per_device(): lax.all_gather(recurrence_branch_weight, 'fs', axis=0, tiled=True)]
    all_to_all x0 -> x1, starting transfers between devices: none -> 8.52 us  [per_device(): lax.all_to_all(jnp.stack([mixer_output_weight] * lax.axis_size('fs')), 'f...]
    all_gather x1, waiting for transfers between devices: 9.07 us -> 0.68 us  [per_device(): whole_rows = lax.all_gather(tokens, 'tp', axis=1, tiled=True)]
  transfers between devices with their start and end apart: 9 -> 9, of which waited for: 9 -> 8; matrix products, arithmetic and copies ran while one was open for 4% -> 5% of each run, Pallas kernels for 0% -> 0%
where the time goes in v1:
time: 677 us
  waiting for transfers between devices  606 us (90%)
  matrix products  31.8 us (5%)
  between operations  14.2 us (2%)
  other arithmetic  9.97 us (1%)
  starting transfers between devices  8.98 us (1%)
    all_gather x1, waiting for transfers between devices, per_device(): lax.all_gather(down_projection_weight, 'fs', axis=1, tiled=True)  172 us
    all_gather x1, waiting for transfers between devices, per_device(): lax.all_gather(value_up_weight, 'fs', axis=0, tiled=True)  143 us
    all_gather x1, waiting for transfers between devices, per_device(): lax.all_gather(gate_up_weight, 'fs', axis=0, tiled=True)  135 us
    all_gather x1, waiting for transfers between devices, per_device(): lax.all_gather(recurrence_branch_weight, 'fs', axis=0, tiled=True)  75 us
    all_gather x1, waiting for transfers between devices, per_device(): lax.all_gather(output_gate_projection, 'fs', axis=0, tiled=True)  53 us
    psum x1, waiting for transfers between devices, per_device(): lax.psum(mixer_terms.astype(jnp.bfloat16), 'tp').astype(jnp.float32)  16 us
  transfers between devices with their start and end apart: 9, of which 8 were waited for; matrix products, arithmetic and copies ran while one was open for 5% of the time, Pallas kernels for 0%

profile of v1, /device:TPU:0, one launch (start us, length us, event | category | flops | bytes accessed | tf_op | source)
XLA Modules:
  0.0 676.8 jit_solution(4494079024308303993)
XLA Ops:
  6.5 0.7 all-gather.7.cloned.1.call-update
  7.3 0.0 all-gather.9.cloned.1.call-start
  7.3 0.7 all-gather.9.cloned.1.call-update
  8.0 1.0 copy.28
  9.0 1.6 stack.2
  10.6 8.5 %all-to-all-start = ((bf16[16,512,128]{1,2,0:T(8,128)(2,1)}), bf16[16,512,128]{1,2,0:T(8,128)(2,1)}, u32[]{:S(2)}, u32[]{:S(2)}) async-start(bf16[16,512,128]{1,2,0:T(8,128)(2,1)} %stack.2), calls=%async_computation | async-start | bytes 4194304 | tf_op jit(solution)/shard_map/all_to_all | solution.py:99
  19.1 0.0 all-gather.11.cloned.1.call-start
  19.2 0.7 all-gather.11.cloned.1.call-update
  19.9 0.0 all-reduce.17.cloned.1.call-start
  20.0 0.7 all-gather.7.cloned.1.call-done
  20.7 1.5 fusion.15
  22.2 75.0 %all-gather.9.cloned.1.call-done = bf16[2048,512]{1,0:T(8,128)(2,1)} async-done(((bf16[128,512]{1,0:T(8,128)(2,1)}), bf16[2048,512]{1,0:T(8,128)(2,1)}) %all-gather.9.cloned.1.call-update) | async-done | bytes 2097168 | tf_op jit(solution)/shard_map/all_gather | solution.py:68
  97.2 2.7 convolution_convert_fusion.5
  99.9 0.1 convert.14
  99.9 0.2 fusion.30
  100.2 0.3 convert_element_type.200
  100.4 0.3 copy.22
  100.8 0.4 fusion.22
  101.2 0.2 copy.24
  101.4 0.4 fusion.24
  101.7 0.2 copy.27
  101.9 0.3 copy-done.5
  102.2 0.4 fusion.52
  102.6 0.1 slice.199
  102.8 0.1 slice.200
  103.0 0.1 slice.198
  103.1 0.1 slice.202
  103.3 0.1 fusion.64
  104.2 0.1 slice.203
  104.3 0.1 slice.236
  104.3 0.2 slice.238
  104.5 0.2 slice.197
  104.8 0.1 pad.52
  104.9 0.1 pad.51
  105.4 0.1 pad.57
  105.5 0.1 pad.58
  105.6 0.1 pad.60
  105.8 0.1 fusion.47
  105.9 0.1 pad.59
  106.0 0.1 add.183
  106.1 53.0 %all-gather.11.cloned.1.call-done = bf16[2048,512]{1,0:T(8,128)(2,1)} async-done(((bf16[128,512]{1,0:T(8,128)(2,1)}), bf16[2048,512]{1,0:T(8,128)(2,1)}) %all-gather.11.cloned.1.call-update) | async-done | bytes 2097168 | tf_op jit(solution)/shard_map/all_gather | solution.py:69
  159.2 4.7 convolution_convert_fusion.3
  163.9 0.0 all-gather.15.cloned.1.call-start
  163.9 0.5 all-gather.15.cloned.1.call-update
  164.5 0.5 all-gather.13.cloned.1.call-update
  165.0 0.0 all-gather.17.cloned.1.call-start
  165.1 0.7 all-gather.17.cloned.1.call-update
  165.8 0.2 reduce-scatter.2.cloned.1.call-start
  166.1 0.1 convert_reduce_fusion.2
  166.2 0.1 convert_reduce_fusion.5
  166.3 16.0 %all-reduce.17.cloned.1.call-done = bf16[256,2048]{1,0:T(8,128)(2,1)} async-done(((bf16[256,2048]{1,0:T(8,128)(2,1)}), bf16[256,2048]{1,0:T(8,128)(2,1)}) %all-reduce.17.cloned.1.call-update) | async-done | bytes 1048592 | tf_op jit(solution)/shard_map/psum | solution.py:105
  182.3 1.7 fusion.12
  184.0 143.5 %all-gather.15.cloned.1.call-done = bf16[2048,2816]{1,0:T(8,128)(2,1)} async-done(((bf16[128,2816]{1,0:T(8,128)(2,1)}), bf16[2048,2816]{1,0:T(8,128)(2,1)}) %all-gather.15.cloned.1.call-update) | async-done | bytes 11534352 | tf_op jit(solution)/shard_map/all_gather | solution.py:110
  327.5 7.5 %convolution_convert_fusion = bf16[256,2816]{1,0:T(8,128)(2,1)S(1)} fusion(bf16[2048,2816]{1,0:T(8,128)(2,1)} %all-gather.15.cloned.1.call-done, bf16[256,2048]{1,0:T(8,128)(2,1)S(1)} %get-tuple-element.12, f32[2048]{0:T(1024)S(1)} %convert_element_type.211, f32[256]{0:T(256)S(1)} %add_rsqrt_fusion), kind=kOutput, calls=%fused_computation | convolution fusion | flops 2955608064 | bytes 14033920 | tf_op jit(solution)/shard_map/dot_general | solution.py:113
  335.0 0.2 convert.16
  335.2 134.5 %all-gather.13.cloned.1.call-done = bf16[2048,2816]{1,0:T(8,128)(2,1)} async-done(((bf16[128,2816]{1,0:T(8,128)(2,1)}), bf16[2048,2816]{1,0:T(8,128)(2,1)}) %all-gather.13.cloned.1.call-update) | async-done | bytes 11534352 | tf_op jit(solution)/shard_map/all_gather | solution.py:109
  469.8 7.8 %convolution_convert_fusion.1 = bf16[256,2816]{1,0:T(8,128)(2,1)S(1)} fusion(bf16[2048,2816]{1,0:T(8,128)(2,1)} %all-gather.13.cloned.1.call-done, bf16[256,2048]{1,0:T(8,128)(2,1)} %copy-done.3, f32[2048]{0:T(1024)S(1)} %convert_element_type.211, f32[256]{0:T(256)S(1)} %add_rsqrt_fusion), kind=kOutput, calls=%fused_computation.1 | convolution fusion | flops 2955608064 | bytes 14033920 | tf_op jit(solution)/shard_map/dot_general | solution.py:112
  477.6 0.2 convert.15
  477.8 1.8 fusion.2
  479.6 0.8 fusion.8
  480.4 172.3 %all-gather.17.cloned.1.call-done = bf16[2816,2048]{1,0:T(8,128)(2,1)} async-done(((bf16[2816,128]{1,0:T(8,128)(2,1)}), bf16[2816,2048]{1,0:T(8,128)(2,1)}) %all-gather.17.cloned.1.call-update) | async-done | bytes 11534352 | tf_op jit(solution)/shard_map/all_gather | solution.py:122
  652.7 8.5 %convolution_convert_fusion.2 = bf16[256,2048]{1,0:T(8,128)(2,1)} fusion(bf16[256,2816]{1,0:T(8,128)(2,1)S(1)} %fusion.8, bf16[2816,2048]{1,0:T(8,128)(2,1)} %all-gather.17.cloned.1.call-done), kind=kOutput, calls=%fused_computation.26 | convolution fusion | flops 2953314304 | bytes 14024704 | tf_op jit(solution)/shard_map/dot_general | solution.py:120
  661.2 6.7 reduce-scatter.2.cloned.1.call-done
  667.9 2.0 add_convert_fusion
  (83 shorter events, 1.4 us)
Async XLA Ops:
  6.5 94.2 %copy-start = (bf16[8,64,64]{2,1,0:T(8,128)(2,1)S(1)}, bf16[8,64,64]{2,1,0:T(8,128)(2,1)}, u32[]{:S(2)}) copy-start(bf16[8,64,64]{2,1,0:T(8,128)(2,1)} %param.21) | copy-start | bytes 196612
  6.5 14.1 %all-gather.7.cloned.1.call-start = ((), (), s32[]{:S(2)}) async-start(), calls=%async_computation.2 | async-start | bytes 1572864 | tf_op jit(solution)/shard_map/all_gather | solution.py:63
  7.3 89.9 %all-gather.9.cloned.1.call-start = ((), (), s32[]{:S(2)}) async-start(), calls=%async_computation.3 | async-start | bytes 2228224 | tf_op jit(solution)/shard_map/all_gather | solution.py:68
  10.6 9.3 %copy-start.9 = (bf16[2048]{0:T(1024)(128)(2,1)S(1)}, bf16[2048]{0:T(1024)(128)(2,1)}, u32[]{:S(2)}) copy-start(bf16[2048]{0:T(1024)(128)(2,1)} %param.17) | copy-start | bytes 12292
  10.6 9.3 %copy-start.8 = (bf16[4,512]{1,0:T(4,128)(2,1)S(1)}, bf16[4,512]{1,0:T(4,128)(2,1)}, u32[]{:S(2)}) copy-start(bf16[4,512]{1,0:T(4,128)(2,1)} %param.20) | copy-start | bytes 12292
  10.6 9.4 %copy-start.11 = (f32[512]{0:T(512)S(1)}, f32[512]{0:T(512)}, u32[]{:S(2)}) copy-start(f32[512]{0:T(512)} %param.23) | copy-start | bytes 6148
  10.6 95.5 %all-to-all-start = ((bf16[16,512,128]{1,2,0:T(8,128)(2,1)}), bf16[16,512,128]{1,2,0:T(8,128)(2,1)}, u32[]{:S(2)}, u32[]{:S(2)}) async-start(bf16[16,512,128]{1,2,0:T(8,128)(2,1)} %stack.2), calls=%async_computation | async-start | bytes 4194304 | tf_op jit(solution)/shard_map/all_to_all | solution.py:99
  19.1 140.0 %all-gather.11.cloned.1.call-start = ((), (), s32[]{:S(2)}) async-start(), calls=%async_computation.4 | async-start | bytes 2228224 | tf_op jit(solution)/shard_map/all_gather | solution.py:69
  19.9 162.4 %all-reduce.17.cloned.1.call-start = ((), (), s32[]{:S(2)}) async-start(), calls=%async_computation.5 | async-start | bytes 2097152 | tf_op jit(solution)/shard_map/psum | solution.py:105
  100.4 0.9 copy-start.12
  101.1 1.1 copy-start.5
  105.8 53.4 %copy-start.2 = (bf16[256,2048]{1,0:T(8,128)(2,1)S(1)}, bf16[256,2048]{1,0:T(8,128)(2,1)}, u32[]{:S(2)}) copy-start(bf16[256,2048]{1,0:T(8,128)(2,1)} %all-gather.7.cloned.1.call-done) | copy-start | bytes 3145732
  163.8 2.2 copy-start.10
  163.9 2.2 copy-start.6
  163.9 2.3 copy-start.7
  163.9 163.6 %all-gather.15.cloned.1.call-start = ((), (), s32[]{:S(2)}) async-start(), calls=%async_computation.7 | async-start | bytes 12255232 | tf_op jit(solution)/shard_map/all_gather | solution.py:110
  164.5 305.3 %all-gather.13.cloned.1.call-start = ((), (), s32[]{:S(2)}) async-start(), calls=%async_computation.6 | async-start | bytes 12255232 | tf_op jit(solution)/shard_map/all_gather | solution.py:109
  165.0 487.7 %all-gather.17.cloned.1.call-start = ((), (), s32[]{:S(2)}) async-start(), calls=%async_computation.8 | async-start | bytes 12255232 | tf_op jit(solution)/shard_map/all_gather | solution.py:122
  165.8 502.1 %reduce-scatter.2.cloned.1.call-start = ((), (), s32[]{:S(2)}) async-start(), calls=%async_computation.9 | async-start | bytes 1572864 | tf_op jit(solution)/shard_map/reduce_scatter | solution.py:126
  184.0 151.0 %copy-start.3 = (bf16[256,2048]{1,0:T(8,128)(2,1)}, bf16[256,2048]{1,0:T(8,128)(2,1)S(1)}, u32[]{:S(2)}) copy-start(bf16[256,2048]{1,0:T(8,128)(2,1)S(1)} %get-tuple-element.12) | copy-start | bytes 3145732
  480.4 187.5 %copy-start.4 = (bf16[256,2048]{1,0:T(8,128)(2,1)S(1)}, bf16[256,2048]{1,0:T(8,128)(2,1)}, u32[]{:S(2)}) copy-start(bf16[256,2048]{1,0:T(8,128)(2,1)} %copy-done.3) | copy-start | bytes 3145732
  652.7 17.2 %copy-start.1 = (bf16[8,64,64]{2,1,0:T(8,128)(2,1)S(1)}, bf16[8,64,64]{2,1,0:T(8,128)(2,1)}, u32[]{:S(2)}) copy-start(bf16[8,64,64]{2,1,0:T(8,128)(2,1)} %param.21) | copy-start | bytes 196612
Sparse Core Ops, SparseCore 0:
  8.9 11.7 all-gather.6
  23.4 73.6 all-gather.8
  99.9 59.1 all-gather.10
  164.0 18.2 all-reduce.16
  184.9 142.6 all-gather.14
  330.1 139.5 all-gather.12
  472.5 180.2 all-gather.16
  661.3 6.5 reduce-scatter.1
